TPU v7x, 256 devices: a 4x2x16 block of a 4x16x16 slice. The times are simulated.
256 devices in a mesh: grp: 2 (over y), sp: 32 (over z, core), tp: 4 (over x).
Axes of the slice: x: 4, y: 2, z: 16, core: 2. Of those that a mesh axis runs over, the one named last changes fastest.
The devices are a block of a 4x16x16 slice.
Arguments:
- residual_in: bfloat16 [16384, 2048], P(('grp', 'sp', 'tp')), parts along dimension 0, may hold values from -1.1953125 to 1.1953125
- query_small: bfloat16 [16384, 1024], P(('grp', 'sp'), 'tp'), parts along dimension 0, may hold values from -6 to 6
- query_large: bfloat16 [16384, 1024], P(('grp', 'sp'), 'tp'), parts along dimension 0, may hold values from -6 to 6
- key_small: bfloat16 [64, 16384], P(None, ('grp', 'sp')), parts along dimension 1, may hold values from -6 to 6
- key_large: bfloat16 [128, 16384], P(None, ('grp', 'sp')), parts along dimension 1, may hold values from -6 to 6
- value_small: bfloat16 [64, 16384], P(None, ('grp', 'sp')), parts along dimension 1, may hold values from -6 to 6
- value_large: bfloat16 [128, 16384], P(None, ('grp', 'sp')), parts along dimension 1, may hold values from -6 to 6
- forget_small: float32 [16, 16384], P('tp', ('grp', 'sp')), parts along dimension 1, may hold values from -1172 to 0, as said below
- forget_large: float32 [8, 16384], P('tp', ('grp', 'sp')), parts along dimension 1, may hold values from -1172 to 0, as said below
- project_small: bfloat16 [1024, 2048], P('tp'), may hold values from -0.125 to 0.125
- project_large: bfloat16 [1024, 2048], P('tp'), may hold values from -0.125 to 0.125
- norm_gain: bfloat16 [2048], replicated, may hold values from 0.099609375 to 1.8984375
- expert_gate: bfloat16 [128, 2048, 512], P(('sp', 'tp')), may hold values from -0.125 to 0.125
- expert_up: bfloat16 [128, 2048, 512], P(('sp', 'tp')), may hold values from -0.125 to 0.125
- expert_down: bfloat16 [128, 512, 2048], P(('sp', 'tp')), may hold values from -0.25 to 0.25
- routing: int32 [16384, 2], P(('grp', 'sp', 'tp')), parts along dimension 0, may hold values from 0 to 127, all different within a row; in each aligned block of 64 rows (0 to 63, 64 to 127, ...) at most 2 rows name the same one
- route_weight: float32 [16384, 2], P(('grp', 'sp', 'tp')), parts along dimension 0, may hold values from 0.2 to 1
Outputs:
- layer_out: bfloat16 [16384, 2048], P(('grp', 'sp', 'tp')), parts along dimension 0
There are 2 independent parts, one for each index of `grp`. A program takes and returns all parts, laid end to end along the dimension named above; an argument that names none is the same for every part. Nothing has to cross between parts.
Inputs may be any that keep to these rules, and one draw needn't show every extreme that they name: `forget_small`: each row never rises from one position to the next. `forget_large`: each row never rises from one position to the next. `routing`: each row names 2 different experts; in the rows of one device no expert is named by more than 2 rows, and in some devices' rows some expert is named by exactly 2.
All inputs are finite; a program needn't handle non-finite values.
Results may differ from a plain program's by a relative error of at most 0.018.
Values may be sent and summed in bfloat16 or wider, within the bound.
No kernel may reach another device: no remote copies, remote signals or barrier semaphores. Data moves between devices by JAX's collectives and lax.ppermute only.
A program may use at most 64 MiB of HBM per device.

v0:
```python
import math

import jax
import jax.numpy as jnp
from jax import lax
from jax.sharding import PartitionSpec as P


def in_one_piece(arrays, axis, dim, along):
    ends, at = ([], 0)
    for a in arrays[:-1]:
        at += a.shape[along]
        ends.append(at)
    both = jnp.concatenate(arrays, axis=along)
    return tuple(jnp.split(lax.all_gather(both, axis, axis=dim, tiled=True), ends, axis=along))


def split_up(value, dim, length):
    shape = value.shape
    parts = value.reshape(*shape[:dim], length, shape[dim] // length, *shape[dim + 1 :])
    return jnp.moveaxis(parts, dim, 0)


def sum_at_owner(value, axis, dim):
    parts = split_up(value, dim, lax.axis_size(axis))
    arrived = lax.all_to_all(parts, axis, split_axis=0, concat_axis=0, tiled=True)
    return arrived.astype(jnp.float32).sum(axis=0)


def softmax_step(
    state, queries, query_gates, query_pos, keys_block, values_block, key_gates, key_pos
):
    row_top, row_total, accum = state
    head_size = keys_block.shape[0]
    scores = jnp.einsum(
        "qhd,dk->hqk", queries, keys_block, preferred_element_type=jnp.float32
    ) * head_size ** (-0.5)
    scores = scores + query_gates[:, :, None] - key_gates[:, None, :]
    causal = (query_pos[:, None] >= key_pos[None, :])[None]
    block_top = jnp.max(jnp.where(causal, scores, -jnp.inf), axis=2)
    new_top = jnp.maximum(row_top, block_top)
    weights = jnp.exp(jnp.where(causal, scores - new_top[:, :, None], -jnp.inf))
    factor = jnp.exp(row_top - new_top)
    new_total = row_total * factor + jnp.sum(weights, axis=2)
    mixed = jnp.einsum(
        "hqk,dk->qhd",
        weights.astype(jnp.bfloat16),
        values_block,
        preferred_element_type=jnp.float32,
    )
    new_accum = accum * factor.T[:, :, None] + mixed
    return (new_top, new_total, new_accum)


def finish(state):
    row_top, row_total, accum = state
    mixed = accum / row_total.T[:, :, None]
    return mixed.reshape(mixed.shape[0], -1).astype(jnp.bfloat16)


def shards(
    residual_in,
    query_small,
    query_large,
    key_small,
    key_large,
    value_small,
    value_large,
    forget_small,
    forget_large,
    project_small,
    project_large,
    norm_gain,
    expert_gate,
    expert_up,
    expert_down,
    routing,
    route_weight,
):
    seq_devices = lax.axis_size("sp")
    seq_index = lax.axis_index("sp")
    head_devices = lax.axis_size("tp")
    local_tokens = query_small.shape[0]
    size_small = key_small.shape[0]
    size_large = key_large.shape[0]
    heads_small = forget_small.shape[0]
    heads_large = forget_large.shape[0]
    model_width = residual_in.shape[1]
    gates_all_small, gates_all_large = in_one_piece((forget_small, forget_large), "sp", 1, 0)
    query_pos = seq_index * local_tokens + jnp.arange(local_tokens)
    group_data = []
    init_states = []
    group_data.append(
        (
            query_small.reshape(local_tokens, heads_small, size_small),
            forget_small,
            query_large.reshape(local_tokens, heads_large, size_large),
            forget_large,
            query_pos,
            jnp.max(query_pos),
        )
    )
    init_states.append(
        (
            jnp.full((heads_small, local_tokens), -1e30, jnp.float32),
            jnp.zeros((heads_small, local_tokens), jnp.float32),
            jnp.zeros((local_tokens, heads_small, size_small), jnp.float32),
            jnp.full((heads_large, local_tokens), -1e30, jnp.float32),
            jnp.zeros((heads_large, local_tokens), jnp.float32),
            jnp.zeros((local_tokens, heads_large, size_large), jnp.float32),
        )
    )
    init_states = tuple(init_states)
    keys_sm, values_sm, keys_lg, values_lg = in_one_piece(
        (key_small, value_small, key_large, value_large), "sp", 1, 0
    )
    piece_len = keys_sm.shape[1]
    sub_len = math.gcd(piece_len, 512)

    def one_sub(sub_index, running):
        local_start = sub_index * sub_len
        block_ks = lax.dynamic_slice_in_dim(keys_sm, local_start, sub_len, 1)
        block_vs = lax.dynamic_slice_in_dim(values_sm, local_start, sub_len, 1)
        block_kl = lax.dynamic_slice_in_dim(keys_lg, local_start, sub_len, 1)
        block_vl = lax.dynamic_slice_in_dim(values_lg, local_start, sub_len, 1)
        block_gs = lax.dynamic_slice_in_dim(gates_all_small, local_start, sub_len, 1)
        block_gl = lax.dynamic_slice_in_dim(gates_all_large, local_start, sub_len, 1)
        key_pos = local_start + jnp.arange(sub_len)
        group = group_data[0]

        def compute(state, group=group):
            new_small = softmax_step(
                state[0:3], group[0], group[1], group[4], block_ks, block_vs, block_gs, key_pos
            )
            new_large = softmax_step(
                state[3:6], group[2], group[3], group[4], block_kl, block_vl, block_gl, key_pos
            )
            return new_small + new_large

        def unchanged(state):
            return state

        updated = [lax.cond(group[5] >= local_start, compute, unchanged, running[0])]
        return tuple(updated)

    final_states = lax.fori_loop(0, piece_len // sub_len, one_sub, init_states)
    attn_small = jnp.concatenate([finish(state[0:3]) for state in final_states], axis=0)
    attn_large = jnp.concatenate([finish(state[3:6]) for state in final_states], axis=0)
    own_rows = local_tokens // head_devices
    total = jnp.dot(attn_small, project_small, preferred_element_type=jnp.float32)
    projected = sum_at_owner(
        (total + jnp.dot(attn_large, project_large, preferred_element_type=jnp.float32)).astype(
            jnp.bfloat16
        ),
        "tp",
        0,
    )
    resid = residual_in.astype(jnp.float32) + projected
    scale = lax.rsqrt(jnp.mean(resid * resid, axis=1, keepdims=True) + 1e-06)
    normed = (resid * scale * norm_gain.astype(jnp.float32)).astype(jnp.bfloat16)
    experts = seq_devices * head_devices
    top_count = routing.shape[1]
    capacity = max(2, 2 * own_rows * top_count // experts)
    pair_count = own_rows * top_count
    pair_expert = routing.reshape(-1)
    one_hot = (pair_expert[:, None] == jnp.arange(experts, dtype=jnp.int32)[None, :]).astype(
        jnp.int32
    )
    earlier = jnp.cumsum(one_hot, axis=0) - one_hot
    slot_of_pair = jnp.sum(earlier * one_hot, axis=1)
    destination = pair_expert * capacity + slot_of_pair
    pair_token = jnp.arange(pair_count) // top_count
    outgoing = jnp.zeros((experts * capacity, model_width), jnp.bfloat16)
    outgoing = (
        outgoing.at[destination].set(normed[pair_token]).reshape(experts, capacity, model_width)
    )
    arrived = lax.all_to_all(outgoing, ("sp", "tp"), split_axis=0, concat_axis=0, tiled=True)
    flat_rows = arrived.reshape(-1, model_width)
    gate_part = jnp.dot(flat_rows, expert_gate[0], preferred_element_type=jnp.float32)
    up_part = jnp.dot(flat_rows, expert_up[0], preferred_element_type=jnp.float32)
    hidden = (jax.nn.silu(gate_part) * up_part).astype(jnp.bfloat16)
    result = jnp.dot(hidden, expert_down[0], preferred_element_type=jnp.float32).astype(
        jnp.bfloat16
    )
    returned = lax.all_to_all(
        result.reshape(arrived.shape), ("sp", "tp"), split_axis=0, concat_axis=0, tiled=True
    )
    picked = returned.reshape(experts * capacity, model_width)[destination]
    weighted = picked.astype(jnp.float32) * route_weight.reshape(-1)[:, None]
    moe_sum = jnp.sum(weighted.reshape(own_rows, top_count, model_width), axis=1)
    return (resid + moe_sum).astype(jnp.bfloat16)


def solution(mesh):
    in_specs = (
        P(("grp", "sp", "tp"), None),
        P(("grp", "sp"), "tp"),
        P(("grp", "sp"), "tp"),
        P(None, ("grp", "sp")),
        P(None, ("grp", "sp")),
        P(None, ("grp", "sp")),
        P(None, ("grp", "sp")),
        P("tp", ("grp", "sp")),
        P("tp", ("grp", "sp")),
        P("tp", None),
        P("tp", None),
        P(),
        P(("sp", "tp"), None, None),
        P(("sp", "tp"), None, None),
        P(("sp", "tp"), None, None),
        P(("grp", "sp", "tp"), None),
        P(("grp", "sp", "tp"), None),
    )
    out_specs = P(("grp", "sp", "tp"), None)
    return jax.shard_map(shards, mesh=mesh, in_specs=in_specs, out_specs=out_specs, check_vma=False)
```

profile of v0, /device:TPU:33, one launch (start us, length us, event | category | flops | bytes accessed | tf_op | source)
XLA Modules:
  0.0 422.0 jit_solution(2980017023659769954)
XLA Ops:
  6.6 1.7 pad_maximum_fusion
  9.0 51.3 %all_gather.7 = f32[6,8192]{1,0:T(8,128)S(1)} all-gather(f32[6,256]{1,0:T(8,128)S(1)} %pad_maximum_fusion.1), channel_id=1, replica_groups=mesh['grp'=2,'sp'=32,'tp'=4] {'sp'}, dimensions={1}, use_global_device_ids=true | all-gather | bytes 202752 | tf_op jit(solution)/shard_map/all_gather | solution.py:15
  65.1 45.0 %all-gather.2.cloned.1.call-done = bf16[384,8192]{1,0:T(8,128)(2,1)} async-done(((bf16[384,256]{1,0:T(8,128)(2,1)}), bf16[384,8192]{1,0:T(8,128)(2,1)}) %all-gather.2.cloned.1.call-update) | async-done | bytes 6291472 | tf_op jit(solution)/shard_map/all_gather | solution.py:15
  110.2 4.7 %fusion.63 = (bf16[128,8192]{1,0:T(8,128)(2,1)}, bf16[128,8192]{1,0:T(8,128)(2,1)}) fusion(bf16[384,8192]{1,0:T(8,128)(2,1)} %all-gather.2.cloned.1.call-done), kind=kLoop, calls=%fused_computation.100 | loop fusion | bytes 8388608 | tf_op jit(solution)/shard_map/split | solution.py:15
  114.8 4.1 copy.29
  118.9 3.0 fusion.64
  122.1 18.4 %while.24 = (s32[]{:T(128)}, f32[4,256]{1,0:T(4,128)S(1)}, f32[4,256]{1,0:T(4,128)S(1)}, f32[256,4,64]{0,2,1:T(8,128)S(1)}, f32[2,256]{1,0:T(2,128)S(1)}, /*inde...) while((s32[]{:T(128)}, f32[4,256]{1,0:T(4,128)S(1)}, ...), condition=%wide.region_8.9_spmd.clone, body=%wide.region_1.8_spmd.clone.sunk | while | flops 277484800 | bytes 12212769 | solution.py:146
  122.8 6.6 %conditional.3 = ((f32[4,256]{1,0:T(4,128)S(1)}, f32[4,256]{1,0:T(4,128)S(1)}, f32[256,4,64]{0,2,1:T(8,128)S(1)}, f32[2,256]{1,0:T(2,128)S(1)}, f32[2,256]{1,0:T(2,128)S(1)}, /*index=5*/f32[256,2,128]{2,0,1:T(8,128)S(1)})) conditional(s32[]{:T(128)} %convert_element_type.107, (f32[4,256]{1,0:T(4,128)S(1)}, f32[4,256]{1,0:T(4,128)S(1)}, ...), branch_computations={%region_2.0_spmd, %region_3.7_spmd} | conditional | flops 277484800 | bytes 12209274 | solution.py:143
  126.0 1.5 select_reduce_fusion
  140.7 1.8 fusion.65
  143.9 4.0 all-to-all-start
  148.4 14.2 %all-to-all-done = bf16[4,64,2048]{2,1,0:T(8,128)(2,1)S(1)} async-done(((bf16[4,64,2048]{2,1,0:T(8,128)(2,1)}), bf16[4,64,2048]{2,1,0:T(8,128)(2,1)S(1)}, u32[]{:S(2)}, u32[]{:S(2)}) %all-to-all-start) | async-done | bytes 1048608 | tf_op jit(solution)/shard_map/all_to_all | solution.py:26
  164.3 3.9 scatter_custom_fusion
  168.3 1.5 reshape.157
  169.8 161.4 %all_to_all.15 = bf16[128,2,2048]{2,1,0:T(2,128)(2,1)S(1)} all-to-all(bf16[128,2,2048]{2,1,0:T(2,128)(2,1)} %reshape.157), channel_id=1, replica_groups=mesh['grp'=2,'sp'=32,'tp'=4] {'sp','tp'}, dimensions={0} | all-to-all | bytes 2097152 | tf_op jit(solution)/shard_map/all_to_all | solution.py:177
  332.4 3.5 fusion.40
  335.9 4.0 convolution_convert_fusion
  340.0 2.6 reshape.159
  342.5 8.5 %all-to-all-start.2 = ((bf16[128,2,2048]{2,1,0:T(2,128)(2,1)}), bf16[128,2,2048]{2,1,0:T(2,128)(2,1)}, u32[]{:S(2)}, u32[]{:S(2)}) async-start(bf16[128,2,2048]{2,1,0:T(2,128)(2,1)} %reshape.159), calls=%async_computation.2 | async-start | bytes 2097152 | tf_op jit(solution)/shard_map/all_to_all | solution.py:185
  351.1 54.5 %all-to-all-done.2 = bf16[128,2,2048]{2,1,0:T(2,128)(2,1)} async-done(((bf16[128,2,2048]{2,1,0:T(2,128)(2,1)}), bf16[128,2,2048]{2,1,0:T(2,128)(2,1)}, u32[]{:S(2)}, u32[]{:S(2)}) %all-to-all-start.2) | async-done | bytes 1048608 | tf_op jit(solution)/shard_map/all_to_all | solution.py:185
  405.7 1.5 reshape.160
  407.1 1.7 gather_fusion
  408.9 2.7 reshape.161
  411.6 2.8 multiply_reduce_fusion
  (122 shorter events, 16.8 us)
Async XLA Ops:
  6.5 329.4 %copy-start = (bf16[1,512,2048]{2,1,0:T(8,128)(2,1)S(1)}, bf16[1,512,2048]{2,1,0:T(8,128)(2,1)}, u32[]{:S(2)}) copy-start(bf16[1,512,2048]{2,1,0:T(8,128)(2,1)} %param.35) | copy-start | bytes 6291460
  6.6 103.6 %all-gather.2.cloned.1.call-start = ((), (), s32[]{:S(2)}) async-start(), calls=%async_computation.3 | async-start | bytes 6488064 | tf_op jit(solution)/shard_map/all_gather | solution.py:15
  118.9 3.1 copy-start.6
  118.9 3.2 copy-start.8
  140.6 1.8 copy-start.5
  143.9 4.0 copy-start.7
  143.9 18.8 %copy-start.3 = (bf16[64,2048]{1,0:T(8,128)(2,1)S(1)}, bf16[64,2048]{1,0:T(8,128)(2,1)}, u32[]{:S(2)}) copy-start(bf16[64,2048]{1,0:T(8,128)(2,1)} %param.21) | copy-start | bytes 786436
  143.9 18.6 %all-to-all-start = ((bf16[4,64,2048]{2,1,0:T(8,128)(2,1)}), bf16[4,64,2048]{2,1,0:T(8,128)(2,1)S(1)}, u32[]{:S(2)}, u32[]{:S(2)}) async-start(bf16[4,64,2048]{2,1,0:T(8,128)(2,1)} %bitcast.76), calls=%async_computation | async-start | bytes 2097152 | tf_op jit(solution)/shard_map/all_to_all | solution.py:26
  162.7 0.8 copy-start.1
  332.4 3.5 copy-start.4
  340.0 11.1 %copy-start.9 = (f32[64,2]{0,1:T(2,128)S(1)}, f32[64,2]{0,1:T(2,128)}, u32[]{:S(2)}) copy-start(f32[64,2]{0,1:T(2,128)} %param.37) | copy-start | bytes 1540
  342.5 63.1 %all-to-all-start.2 = ((bf16[128,2,2048]{2,1,0:T(2,128)(2,1)}), bf16[128,2,2048]{2,1,0:T(2,128)(2,1)}, u32[]{:S(2)}, u32[]{:S(2)}) async-start(bf16[128,2,2048]{2,1,0:T(2,128)(2,1)} %reshape.159), calls=%async_computation.2 | async-start | bytes 2097152 | tf_op jit(solution)/shard_map/all_to_all | solution.py:185
  408.9 5.5 %copy-start.2 = (f32[64,2048]{1,0:T(8,128)S(1)}, f32[64,2048]{1,0:T(8,128)}, u32[]{:S(2)}) copy-start(f32[64,2048]{1,0:T(8,128)} %copy-done.1) | copy-start | bytes 1572868
Sparse Core Ops, SparseCore 0:
  9.1 101.0 all-gather.1
where the time goes:
time: 425 us; the launch traced here: 422 us
  blocking collectives  213 us (50%)
  waiting for transfers between devices  114 us (27%)
  local copies, waits for them, and re-layouts  31.3 us (7%)
  matrix products  16.4 us (4%)
  between operations  13.7 us (3%)
  starting transfers between devices  12.5 us (3%)
  loops' own time  11.8 us (3%)
  other arithmetic  9.84 us (2%)
    all_to_all x1, blocking collectives, shards(): lax.all_to_all(outgoing, ('sp', 'tp'), split_axis=0, concat_axis=0, tiled...  161 us
    all_to_all x1, waiting for transfers between devices, shards(): lax.all_to_all(result.reshape(arrived.shape), ('sp', 'tp'), split_axis=0,...  54.5 us
    all_gather x1, blocking collectives, in_one_piece(): lax.all_gather(both, axis, axis=dim, tiled=True)  51.3 us
    all_gather x1, waiting for transfers between devices, in_one_piece(): lax.all_gather(both, axis, axis=dim, tiled=True)  45 us
    all_to_all x1, waiting for transfers between devices, sum_at_owner(): lax.all_to_all(parts, axis, split_axis=0, concat_axis=0, tiled=True)  14.2 us
    another operation x1, loops' own time, shards(): final_states = lax.fori_loop(0, piece_len // sub_len, one_sub, init_states)  11.5 us
  transfers between devices with their start and end apart: 3, of which 3 were waited for; matrix products, arithmetic and copies ran while one was open for 1% of the time, Pallas kernels for 0%

commit v1 on v0

v1 whole, which is shorter than its diff:
```python
import math

import jax
import jax.numpy as jnp
from jax import lax
from jax.experimental import pallas as pl
from jax.experimental.pallas import tpu as pltpu
from jax.sharding import PartitionSpec as P

BF = jnp.bfloat16
F32 = jnp.float32
LOG2E = math.log2(math.e)
GATE_ROWS = 16
PIECES = 3


def round16(n):
    return -(-n // 16) * 16


def in_pieces(gates, size):
    left = gates * -(size**0.5)
    rows = []
    for _ in range(PIECES):
        piece = lax.reduce_precision(left, 8, 7)
        rows.append(piece.astype(BF))
        left = left - piece
    stacked = jnp.concatenate(rows, axis=0)
    pad = GATE_ROWS - stacked.shape[0]
    return jnp.concatenate([stacked, jnp.zeros((pad, gates.shape[1]), BF)], axis=0)


def with_selector(queries, heads, size):
    tokens = queries.shape[0]
    per_head = queries.reshape(tokens, heads, size).transpose(1, 0, 2)
    column = jnp.arange(GATE_ROWS)[None, :]
    head = jnp.arange(heads)[:, None]
    chosen = (column % heads == head) & (column < PIECES * heads)
    chosen = jnp.broadcast_to(chosen.astype(BF)[:, None, :], (heads, tokens, GATE_ROWS))
    return jnp.concatenate([per_head, chosen], axis=2)


def attention_body(info, qs, ql, kv, gates, ps, pb, out, m_s, a_s, m_l, t_l, a_l):
    step = pl.program_id(0)
    heads_s, tokens, width_s = qs.shape
    heads_l, _, width_l = ql.shape
    ds, dl = width_s - GATE_ROWS, width_l - GATE_ROWS
    per_step = kv.shape[0]
    keys = per_step * kv.shape[2]
    sp = info[0]
    last = sp // per_step

    @pl.when(step == 0)
    def _():
        m_s[...] = jnp.full_like(m_s, -1e30)
        m_l[...] = jnp.full_like(m_l, -1e30)
        a_s[...] = jnp.zeros_like(a_s)
        a_l[...] = jnp.zeros_like(a_l)
        t_l[...] = jnp.zeros_like(t_l)

    def block(masked):
        def rows_of(ref, first, count):
            return jnp.concatenate([ref[i, first : first + count] for i in range(per_step)], axis=1)

        k_s = jnp.concatenate([rows_of(kv, 0, ds), rows_of(gates, 0, GATE_ROWS)], axis=0)
        v_s = rows_of(kv, ds, ds)
        k_l = jnp.concatenate([rows_of(kv, 2 * ds, dl), rows_of(gates, GATE_ROWS, GATE_ROWS)], axis=0)
        v_l = rows_of(kv, 2 * ds + dl, dl)
        ones = jnp.ones((GATE_ROWS, keys), BF)
        v_s = jnp.concatenate([v_s, ones], axis=0)
        if masked:
            q_pos = lax.broadcasted_iota(jnp.int32, (tokens, keys), 0) + (sp * tokens - step * keys)
            keep = q_pos >= lax.broadcasted_iota(jnp.int32, (tokens, keys), 1)

        def one(q, k, size, m_ref, h):
            s = jnp.dot(q[h], k, preferred_element_type=F32)
            if masked:
                s = jnp.where(keep, s, -1e30)
            top = m_ref[h]
            new = jnp.maximum(top, jnp.max(s, axis=1, keepdims=True))
            m_ref[h] = new
            c = LOG2E * size**-0.5
            return jnp.exp2((s - new) * c), jnp.exp2((top - new) * c)

        for h in range(heads_s):
            p, alpha = one(qs, k_s, ds, m_s, h)
            mixed = lax.dot_general(p.astype(BF), v_s, (((1,), (1,)), ((), ())), preferred_element_type=F32)
            a_s[h] = a_s[h] * alpha + mixed
        for h in range(heads_l):
            p, alpha = one(ql, k_l, dl, m_l, h)
            mixed = lax.dot_general(p.astype(BF), v_l, (((1,), (1,)), ((), ())), preferred_element_type=F32)
            a_l[h] = a_l[h] * alpha + mixed
            t_l[h] = t_l[h] * alpha + jnp.sum(p, axis=1, keepdims=True)

    @pl.when(step < last)
    def _():
        block(False)

    @pl.when(step == last)
    def _():
        block(True)

    @pl.when(step == pl.num_programs(0) - 1)
    def _():
        small = [(a_s[h, :, :ds] / a_s[h, :, ds : ds + 1]).astype(BF) for h in range(heads_s)]
        large = [(a_l[h] / t_l[h]).astype(BF) for h in range(heads_l)]
        total = jnp.dot(jnp.concatenate(small, axis=1), ps[...], preferred_element_type=F32)
        total = total + jnp.dot(jnp.concatenate(large, axis=1), pb[...], preferred_element_type=F32)
        out[...] = total.astype(BF)


def attention(info, qs, ql, kv, gates, ps, pb, per_step=4):
    blocks, _, block_keys = kv.shape
    tokens, width = qs.shape[1], ps.shape[1]
    ds, dl = qs.shape[2] - GATE_ROWS, ql.shape[2] - GATE_ROWS
    step_map = lambda j, i: (jnp.minimum(j, i[0] // per_step), 0, 0)
    whole = lambda a: pl.BlockSpec(a.shape, lambda j, i: (0,) * a.ndim)
    return pl.pallas_call(
        attention_body,
        grid_spec=pltpu.PrefetchScalarGridSpec(
            num_scalar_prefetch=1,
            grid=(blocks // per_step,),
            in_specs=[
                whole(qs),
                whole(ql),
                pl.BlockSpec((per_step,) + kv.shape[1:], step_map),
                pl.BlockSpec((per_step,) + gates.shape[1:], step_map),
                whole(ps),
                whole(pb),
            ],
            out_specs=pl.BlockSpec((tokens, width), lambda j, i: (0, 0)),
            scratch_shapes=[
                pltpu.VMEM((qs.shape[0], tokens, 1), F32),
                pltpu.VMEM((qs.shape[0], tokens, ds + GATE_ROWS), F32),
                pltpu.VMEM((ql.shape[0], tokens, 1), F32),
                pltpu.VMEM((ql.shape[0], tokens, 1), F32),
                pltpu.VMEM((ql.shape[0], tokens, dl), F32),
            ],
        ),
        out_shape=jax.ShapeDtypeStruct((tokens, width), BF),
        compiler_params=pltpu.CompilerParams(dimension_semantics=("arbitrary",), vmem_limit_bytes=60 << 20),
        name="attention",
    )(info, qs, ql, kv, gates, ps, pb)


def mix_body(parts, residual_in, gain, slots, resid_out, outgoing):
    projected = parts[0].astype(F32)
    for i in range(1, parts.shape[0]):
        projected = projected + parts[i].astype(F32)
    resid = residual_in[...].astype(F32) + projected
    resid_out[...] = resid
    scale = lax.rsqrt(jnp.mean(resid * resid, axis=1, keepdims=True) + 1e-06)
    normed = (resid * scale * gain[...].astype(F32)).astype(BF)
    outgoing[...] = jnp.dot(slots[...], normed, preferred_element_type=F32).astype(BF)


def mix(parts, residual_in, gain, slots):
    rows, width = residual_in.shape
    return pl.pallas_call(
        mix_body,
        out_shape=(
            jax.ShapeDtypeStruct((rows, width), F32),
            jax.ShapeDtypeStruct((slots.shape[0], width), BF),
        ),
        compiler_params=pltpu.CompilerParams(vmem_limit_bytes=40 << 20),
        name="mix",
    )(parts, residual_in, gain, slots)


def expert_body(rows, gate, up, down, out, total):
    step = pl.program_id(0)
    x = rows[...]
    g = jnp.dot(x, gate[0], preferred_element_type=F32)
    u = jnp.dot(x, up[0], preferred_element_type=F32)
    hidden = (g / (1.0 + jnp.exp(-g)) * u).astype(BF)
    part = jnp.dot(hidden, down[0], preferred_element_type=F32)

    @pl.when(step == 0)
    def _():
        total[...] = part

    @pl.when(step > 0)
    def _():
        total[...] += part

    @pl.when(step == pl.num_programs(0) - 1)
    def _():
        out[...] = total[...].astype(BF)


def expert(rows, gate, up, down, chunk=128):
    count, width = rows.shape
    units = gate.shape[2]
    return pl.pallas_call(
        expert_body,
        grid=(units // chunk,),
        in_specs=[
            pl.BlockSpec((count, width), lambda i: (0, 0)),
            pl.BlockSpec((1, width, chunk), lambda i: (0, 0, i)),
            pl.BlockSpec((1, width, chunk), lambda i: (0, 0, i)),
            pl.BlockSpec((1, chunk, width), lambda i: (0, i, 0)),
        ],
        out_specs=pl.BlockSpec((count, width), lambda i: (0, 0)),
        out_shape=jax.ShapeDtypeStruct((count, width), BF),
        scratch_shapes=[pltpu.VMEM((count, width), F32)],
        compiler_params=pltpu.CompilerParams(dimension_semantics=("arbitrary",), vmem_limit_bytes=40 << 20),
        name="expert",
    )(rows, gate, up, down)


def collect_body(returned, weights, resid, out):
    total = resid[...]
    for i in range(weights.shape[0]):
        total = total + jnp.dot(weights[i], returned[...], preferred_element_type=F32)
    out[...] = total.astype(BF)


def collect(returned, weights, resid):
    return pl.pallas_call(
        collect_body,
        out_shape=jax.ShapeDtypeStruct(resid.shape, BF),
        compiler_params=pltpu.CompilerParams(vmem_limit_bytes=40 << 20),
        name="collect",
    )(returned, weights, resid)


def three_pieces(value):
    pieces = []
    for _ in range(PIECES):
        piece = lax.reduce_precision(value, 8, 7)
        pieces.append(piece.astype(BF))
        value = value - piece
    return jnp.stack(pieces)


def shards(
    residual_in,
    query_small,
    query_large,
    key_small,
    key_large,
    value_small,
    value_large,
    forget_small,
    forget_large,
    project_small,
    project_large,
    norm_gain,
    expert_gate,
    expert_up,
    expert_down,
    routing,
    route_weight,
):
    head_devices = lax.axis_size("tp")
    experts = lax.axis_size("sp") * head_devices
    size_small, size_large = key_small.shape[0], key_large.shape[0]
    own_rows, width = residual_in.shape
    top_count = routing.shape[1]

    gates = jnp.concatenate([in_pieces(forget_small, size_small), in_pieces(forget_large, size_large)], axis=0)
    packed = jnp.concatenate([key_small, value_small, key_large, value_large], axis=0)
    all_gates = lax.all_gather(gates, "sp", axis=0)
    all_kv = lax.all_gather(packed, "sp", axis=0)

    info = lax.axis_index("sp").astype(jnp.int32).reshape(1)
    partial = attention(
        info,
        with_selector(query_small, forget_small.shape[0], size_small),
        with_selector(query_large, forget_large.shape[0], size_large),
        all_kv,
        all_gates,
        project_small,
        project_large,
    )

    capacity = max(2, 2 * own_rows * top_count // experts)
    pairs = own_rows * top_count
    pair_expert = routing.reshape(-1)
    same = pair_expert[:, None] == pair_expert[None, :]
    before = jnp.arange(pairs)[:, None] > jnp.arange(pairs)[None, :]
    slot = jnp.sum((same & before).astype(jnp.int32), axis=1)
    target = (pair_expert * capacity + slot).reshape(own_rows, top_count)
    hit = target[:, :, None] == jnp.arange(experts * capacity)[None, None, :]
    slots = jnp.any(hit, axis=1).T.astype(BF)
    weights = three_pieces(jnp.sum(jnp.where(hit, route_weight[:, :, None], 0.0), axis=1))

    parts = partial.reshape(head_devices, own_rows, width)
    parts = lax.all_to_all(parts, "tp", split_axis=0, concat_axis=0, tiled=True)
    resid, outgoing = mix(parts, residual_in, norm_gain.reshape(1, width), slots)
    outgoing = outgoing.reshape(experts, capacity, width)
    arrived = lax.all_to_all(outgoing, ("sp", "tp"), split_axis=0, concat_axis=0, tiled=True)
    result = expert(arrived.reshape(-1, width), expert_gate, expert_up, expert_down)
    result = result.reshape(experts, capacity, width)
    returned = lax.all_to_all(result, ("sp", "tp"), split_axis=0, concat_axis=0, tiled=True)
    return collect(returned.reshape(-1, width), weights, resid)


def solution(mesh):
    in_specs = (
        P(("grp", "sp", "tp"), None),
        P(("grp", "sp"), "tp"),
        P(("grp", "sp"), "tp"),
        P(None, ("grp", "sp")),
        P(None, ("grp", "sp")),
        P(None, ("grp", "sp")),
        P(None, ("grp", "sp")),
        P("tp", ("grp", "sp")),
        P("tp", ("grp", "sp")),
        P("tp", None),
        P("tp", None),
        P(),
        P(("sp", "tp"), None, None),
        P(("sp", "tp"), None, None),
        P(("sp", "tp"), None, None),
        P(("grp", "sp", "tp"), None),
        P(("grp", "sp", "tp"), None),
    )
    out_specs = P(("grp", "sp", "tp"), None)
    return jax.shard_map(shards, mesh=mesh, in_specs=in_specs, out_specs=out_specs, check_vma=False)
```

time: 425 us -> 301 us (0.71)
  blocking collectives: 213 us -> 144 us
  local copies, waits for them, and re-layouts: 31.3 us -> 12 us
  waiting for transfers between devices: 114 us -> 97.3 us
  matrix products: 16.4 us -> 0 us
  Pallas kernels: 0 us -> 15.9 us
  loops' own time: 11.8 us -> 0 us
  other arithmetic: 9.84 us -> 4.99 us
    all_to_all x1, blocking collectives: 161 us -> 88.1 us  [shards(): lax.all_to_all(outgoing, ('sp', 'tp'), split_axis=0, concat_axis=0, tiled...]
    dot_general x8 -> x0, matrix products: 16.4 us -> none  [the longest x1 4.01 us: shards(): jnp.dot(hidden, expert_down[0], preferred_element_type=jnp.float32)]
    pallas_call x0 -> x4, Pallas kernels: none -> 15.9 us  [the longest x1 8.09 us: attention(): pl.pallas_call(attention_body, grid_spec=pltpu.PrefetchScalarGridSpec(num...]
    all_gather x1, waiting for transfers between devices: 45 us -> 29.3 us  [shards(): all_kv = lax.all_gather(packed, 'sp', axis=0)]
    another operation x17 -> x0, loops' own time: 11.8 us -> none  [the longest x1 11.5 us: shards(): final_states = lax.fori_loop(0, piece_len // sub_len, one_sub, init_states)]
    split x4 -> x0, local copies, waits for them, and re-layouts: 7.79 us -> none  [in_one_piece(): jnp.split(lax.all_gather(both, axis, axis=dim, tiled=True), ends, axis=al...]
    all_gather x1, blocking collectives: 51.3 us -> 55.7 us  [shards(): all_gates = lax.all_gather(gates, 'sp', axis=0)]
  transfers between devices with their start and end apart: 3 -> 3, of which waited for: 3 -> 3; matrix products, arithmetic and copies ran while one was open for 1% -> 2% of each run, Pallas kernels for 0% -> 0%
where the time goes in v1:
time: 301 us
  blocking collectives  144 us (48%)
  waiting for transfers between devices  97.3 us (32%)
  Pallas kernels  15.9 us (5%)
  between operations  13.7 us (5%)
  starting transfers between devices  13 us (4%)
  local copies, waits for them, and re-layouts  12 us (4%)
  other arithmetic  4.99 us (2%)
    all_to_all x1, blocking collectives, shards(): lax.all_to_all(outgoing, ('sp', 'tp'), split_axis=0, concat_axis=0, tiled...  88.1 us
    all_gather x1, blocking collectives, shards(): all_gates = lax.all_gather(gates, 'sp', axis=0)  55.7 us
    all_to_all x1, waiting for transfers between devices, shards(): lax.all_to_all(result, ('sp', 'tp'), split_axis=0, concat_axis=0, tiled=T...  54.2 us
    all_gather x1, waiting for transfers between devices, shards(): all_kv = lax.all_gather(packed, 'sp', axis=0)  29.3 us
    all_to_all x1, waiting for transfers between devices, shards(): parts = lax.all_to_all(parts, 'tp', split_axis=0, concat_axis=0, tiled=True)  13.7 us
    all_to_all x1, starting transfers between devices, shards(): lax.all_to_all(result, ('sp', 'tp'), split_axis=0, concat_axis=0, tiled=T...  8.49 us
    pallas_call x1, Pallas kernels, attention(): pl.pallas_call(attention_body, grid_spec=pltpu.PrefetchScalarGridSpec(num...  8.09 us
    unnamed x17, local copies, waits for them, and re-layouts  6.89 us
  transfers between devices with their start and end apart: 3, of which 3 were waited for; matrix products, arithmetic and copies ran while one was open for 2% of the time, Pallas kernels for 0%

profile of v1, /device:TPU:33, one launch (start us, length us, event | category | flops | bytes accessed | tf_op | source)
XLA Modules:
  0.0 300.6 jit_solution(4285549265790301999)
XLA Ops:
  6.6 1.5 pad_maximum_fusion.2
  8.2 1.0 copy.39
  9.4 1.0 copy.41
  10.5 0.7 fusion.7
  11.2 0.7 fusion.5
  12.2 0.9 pad_maximum_fusion.qs
  13.1 0.7 pad_maximum_fusion.1.ql
  13.8 55.7 %all-gather.1 = bf16[1024,256]{1,0:T(8,128)(2,1)} all-gather(bf16[32,256]{1,0:T(8,128)(2,1)S(1)} %concatenate.15), channel_id=3, replica_groups=mesh['grp'=2,'sp'=32,'tp'=4] {'sp'}, dimensions={0}, use_global_device_ids=true | all-gather | bytes 540672 | tf_op jit(solution)/shard_map/all_gather | solution.py:263
  69.5 29.3 %all-gather.4.cloned.1.call-done = bf16[12288,256]{1,0:T(8,128)(2,1)} async-done(((bf16[384,256]{1,0:T(8,128)(2,1)}), bf16[12288,256]{1,0:T(8,128)(2,1)}) %all-gather.4.cloned.1.call-update) | async-done | bytes 6291472 | tf_op jit(solution)/shard_map/all_gather | solution.py:264
  98.8 8.1 %attention.1 = bf16[256,2048]{1,0:T(8,128)(2,1)} custom-call(s32[1]{0:T(128)} %bitcast.info, bf16[4,256,80]{2,1,0:T(8,128)(2,1)} %pad_maximum_fusion.qs, bf16[2,256,144]{2,1,0:T(8,128)(2,1)} %pad_maximum_fusion.1.ql, bf16[32,384,256]{2,1,0:T(8,128)(2,1)} %bitcast.17, bf16[32,32,256]{2,1,0:T(8,128)(2,1)} %bitcast.19, bf16[256,2048]{1,0:T(8,128)(2,1)} %ps.1, ...), custom_call_target="tpu_custom_call" | custom-call | tf_op jit(solution)/shard_map/attention/pallas_call | solution.py:118
  106.9 4.5 %all-to-all-start = ((bf16[4,64,2048]{2,1,0:T(8,128)(2,1)}), bf16[4,64,2048]{2,1,0:T(8,128)(2,1)S(1)}, u32[]{:S(2)}, u32[]{:S(2)}) async-start(bf16[4,64,2048]{2,1,0:T(8,128)(2,1)} %bitcast.18), calls=%async_computation | async-start | bytes 2097152 | tf_op jit(solution)/shard_map/all_to_all | solution.py:289
  112.4 13.7 %all-to-all-done.parts = bf16[4,64,2048]{2,1,0:T(8,128)(2,1)S(1)} async-done(((bf16[4,64,2048]{2,1,0:T(8,128)(2,1)}), bf16[4,64,2048]{2,1,0:T(8,128)(2,1)S(1)}, u32[]{:S(2)}, u32[]{:S(2)}) %all-to-all-start) | async-done | bytes 1048608 | tf_op jit(solution)/shard_map/all_to_all | solution.py:289
  126.1 0.7 mix.1
  126.8 0.7 reshape.178
  127.5 88.1 %all_to_all.15 = bf16[128,2,2048]{2,1,0:T(2,128)(2,1)S(1)} all-to-all(bf16[128,2,2048]{2,1,0:T(2,128)(2,1)S(1)} %reshape.178), channel_id=1, replica_groups=mesh['grp'=2,'sp'=32,'tp'=4] {'sp','tp'}, dimensions={0} | all-to-all | bytes 2097152 | tf_op jit(solution)/shard_map/all_to_all | solution.py:292
  216.0 1.6 copy-done
  217.6 1.6 copy-done.1
  219.2 1.6 copy-done.2
  220.8 5.8 %expert.1 = bf16[256,2048]{1,0:T(8,128)(2,1)S(1)} custom-call(bf16[256,2048]{1,0:T(8,128)(2,1)S(1)} %reshape.179.rows, bf16[1,2048,512]{2,1,0:T(8,128)(2,1)S(1)} %copy-done, bf16[1,2048,512]{2,1,0:T(8,128)(2,1)S(1)} %copy-done.1, bf16[1,512,2048]{2,1,0:T(8,128)(2,1)S(1)} %copy-done.2), custom_call_target="tpu_custom_call" | custom-call | tf_op jit(solution)/shard_map/expert/pallas_call | solution.py:194
  226.6 1.5 reshape.180
  228.1 8.5 %all-to-all-start.2 = ((bf16[128,2,2048]{2,1,0:T(2,128)(2,1)}), bf16[128,2,2048]{2,1,0:T(2,128)(2,1)}, u32[]{:S(2)}, u32[]{:S(2)}) async-start(bf16[128,2,2048]{2,1,0:T(2,128)(2,1)} %reshape.180), calls=%async_computation.2 | async-start | bytes 2097152 | tf_op jit(solution)/shard_map/all_to_all | solution.py:295
  236.8 54.2 %all-to-all-done.2 = bf16[128,2,2048]{2,1,0:T(2,128)(2,1)} async-done(((bf16[128,2,2048]{2,1,0:T(2,128)(2,1)}), bf16[128,2,2048]{2,1,0:T(2,128)(2,1)}, u32[]{:S(2)}, u32[]{:S(2)}) %all-to-all-start.2) | async-done | bytes 1048608 | tf_op jit(solution)/shard_map/all_to_all | solution.py:295
  290.9 1.5 reshape.181.returned
  292.4 1.4 collect.1
  (40 shorter events, 2.1 us)
Async XLA Ops:
  6.5 92.3 %all-gather.4.cloned.1.call-start = ((), (), s32[]{:S(2)}) async-start(), calls=%async_computation.3 | async-start | bytes 6488064 | tf_op jit(solution)/shard_map/all_gather | solution.py:264
  106.9 4.5 %copy-start.5 = (s32[64,2]{0,1:T(2,128)S(1)}, s32[64,2]{0,1:T(2,128)}, u32[]{:S(2)}) copy-start(s32[64,2]{0,1:T(2,128)} %param.32) | copy-start | bytes 1540
  106.9 5.4 %copy-start.4 = (bf16[2048]{0:T(1024)(128)(2,1)S(1)}, bf16[2048]{0:T(1024)(128)(2,1)}, u32[]{:S(2)}) copy-start(bf16[2048]{0:T(1024)(128)(2,1)} %param.28) | copy-start | bytes 12292
  106.9 19.2 %copy-start.3 = (bf16[64,2048]{1,0:T(8,128)(2,1)S(1)}, bf16[64,2048]{1,0:T(8,128)(2,1)}, u32[]{:S(2)}) copy-start(bf16[64,2048]{1,0:T(8,128)(2,1)} %residual_in.1) | copy-start | bytes 786436
  106.9 19.2 %all-to-all-start = ((bf16[4,64,2048]{2,1,0:T(8,128)(2,1)}), bf16[4,64,2048]{2,1,0:T(8,128)(2,1)S(1)}, u32[]{:S(2)}, u32[]{:S(2)}) async-start(bf16[4,64,2048]{2,1,0:T(8,128)(2,1)} %bitcast.18), calls=%async_computation | async-start | bytes 2097152 | tf_op jit(solution)/shard_map/all_to_all | solution.py:289
  216.0 1.6 copy-start
  217.6 1.6 copy-start.1
  219.2 1.6 copy-start.2
  226.6 10.0 %copy-start.6 = (f32[64,2]{0,1:T(2,128)S(1)}, f32[64,2]{0,1:T(2,128)}, u32[]{:S(2)}) copy-start(f32[64,2]{0,1:T(2,128)} %param.33) | copy-start | bytes 1540
  228.1 62.9 %all-to-all-start.2 = ((bf16[128,2,2048]{2,1,0:T(2,128)(2,1)}), bf16[128,2,2048]{2,1,0:T(2,128)(2,1)}, u32[]{:S(2)}, u32[]{:S(2)}) async-start(bf16[128,2,2048]{2,1,0:T(2,128)(2,1)} %reshape.180), calls=%async_computation.2 | async-start | bytes 2097152 | tf_op jit(solution)/shard_map/all_to_all | solution.py:295
Sparse Core Ops, SparseCore 0:
  9.2 89.5 all-gather.3
